TPU v7x, 32 devices: a whole 2x2x4 slice. The times are simulated.
32 devices in a mesh: grp: 2 (over y), ep: 4 (over z), tp: 4 (over x, core).
Axes of the slice: x: 2, y: 2, z: 4, core: 2. Of those that a mesh axis runs over, the one named last changes fastest.
Arguments:
- queries: bfloat16 [1024, 2048], P(('grp', 'ep'), 'tp'), parts along dimension 0, may hold values from -6 to 6
- keys: bfloat16 [1024, 2048], P(('grp', 'ep'), 'tp'), parts along dimension 0, may hold values from -6 to 6
- values: bfloat16 [1024, 2048], P(('grp', 'ep'), 'tp'), parts along dimension 0, may hold values from -6 to 6
- stop_bias: bfloat16 [1024, 32], P(('grp', 'ep'), 'tp'), parts along dimension 0, may hold values from -20 to 0
- out_weight: bfloat16 [2048, 2048], P('tp'), may hold values from -0.125 to 0.125
- mix_gain: float32 [2048], replicated, may hold values from 0.1 to 1.9
- moe_input: bfloat16 [4096, 2048], P(('grp', 'ep', 'tp')), parts along dimension 0, may hold values from -6 to 6
- ffn_gain: float32 [2048], replicated, may hold values from 0.1 to 1.9
- expert_ids: int32 [4096, 2], P(('grp', 'ep', 'tp')), parts along dimension 0, may hold values from 0 to 3, all different within a row; in each aligned block of 128 rows (0 to 127, 128 to 255, ...) at most 96 rows name the same one
- expert_scores: float32 [4096, 2], P(('grp', 'ep', 'tp')), parts along dimension 0, may hold values from 0.05 to 1
- gate_weight: bfloat16 [4, 2048, 1024], P('ep', None, 'tp'), may hold values from -0.125 to 0.125
- up_weight: bfloat16 [4, 2048, 1024], P('ep', None, 'tp'), may hold values from -0.125 to 0.125
- down_weight: bfloat16 [4, 1024, 2048], P('ep', 'tp'), may hold values from -0.1875 to 0.1875
Outputs:
- mixed: bfloat16 [1024, 2048], P(('grp', 'ep', 'tp')), parts along dimension 0
- experts_mixed: bfloat16 [4096, 2048], P(('grp', 'ep', 'tp')), parts along dimension 0
There are 2 independent parts, one for each index of `grp`. A program takes and returns all parts, laid end to end along the dimension named above; an argument that names none is the same for every part. Nothing has to cross between parts.
Inputs may be any that keep to these rules, and one draw needn't show every extreme that they name: `expert_ids`: each token names 2 different experts. Among the 128 tokens of one device, no expert is named by more than 96 tokens, and in some device's tokens some expert is named by exactly 96.
All inputs are finite; a program needn't handle non-finite values.
Results may differ from a plain program's by a relative error of at most 0.012.
Values may be sent and summed in bfloat16 or wider, within the bound.
A program may use at most 128 MiB of HBM per device.

v0:
```python
import jax
import jax.numpy as jnp
from jax import lax
from jax.sharding import PartitionSpec as P


def norm_rows(values, gain):
    values = values.astype(jnp.float32)
    scale = lax.rsqrt(jnp.mean(values * values, axis=-1, keepdims=True) + 1e-06)
    return values * scale * gain


def break_terms(query_heads, query_place, key_block, bias_block, first):
    span = key_block.shape[0]
    heads = query_heads.shape[1]
    key_heads = key_block.reshape(span, heads, -1)
    scores = jnp.einsum("qhd,khd->hqk", query_heads, key_heads, preferred_element_type=jnp.float32)
    scores = scores * query_heads.shape[2] ** (-0.5) + bias_block.astype(jnp.float32).T[:, None, :]
    key_place = first + jnp.arange(span)
    past = (key_place[None, :] < query_place[:, None])[None]
    rest = jnp.where(past, jax.nn.log_sigmoid(-scores), 0.0)
    later = lax.cumsum(rest, axis=2, reverse=True)
    return (scores, past, rest, later)


def block_part(scores, past, rest, later, value_block, heads):
    within = later - rest
    local = jnp.where(past, jnp.exp(jax.nn.log_sigmoid(scores) + within), 0.0).astype(jnp.bfloat16)
    span = value_block.shape[0]
    value_heads = value_block.reshape(span, heads, -1)
    part = jnp.einsum("hqk,khd->qhd", local, value_heads, preferred_element_type=jnp.float32)
    return part.reshape(part.shape[0], -1)


def keep(state):
    return state


def dispatch_plan(normed, expert_ids, experts, capacity):
    rows, top = expert_ids.shape
    flat_ids = expert_ids.reshape(rows * top)
    onehot = (flat_ids[:, None] == jnp.arange(experts)[None, :]).astype(jnp.int32)
    earlier = jnp.cumsum(onehot, axis=0) - onehot
    place = jnp.sum(earlier * onehot, axis=1)
    target = flat_ids * capacity + place
    source = (
        jnp.zeros((experts * capacity,), jnp.int32)
        .at[target]
        .set(jnp.arange(rows * top, dtype=jnp.int32) // top + 1)
    )
    padded = jnp.concatenate([jnp.zeros((1, normed.shape[1]), normed.dtype), normed], axis=0)
    return (padded[source].reshape(experts, capacity, normed.shape[1]), target)


def expert_hidden(piece, gate_weight, up_weight):
    flat = piece.reshape(-1, piece.shape[-1])
    gate = jnp.dot(flat, gate_weight[0], preferred_element_type=jnp.float32)
    upward = jnp.dot(flat, up_weight[0], preferred_element_type=jnp.float32)
    hidden = (jax.nn.silu(gate) * upward).astype(jnp.bfloat16)
    return hidden.reshape(piece.shape[0], piece.shape[1], -1)


def send_back(summed):
    return lax.all_to_all(
        summed.astype(jnp.bfloat16), "ep", split_axis=0, concat_axis=0, tiled=True
    )


def return_rows(hidden_all, down_weight, sources):
    flat = hidden_all.reshape(-1, hidden_all.shape[2])
    product = jnp.dot(flat, down_weight[0], preferred_element_type=jnp.float32)
    return send_back(
        lax.psum_scatter(
            product.reshape(sources * lax.axis_size("tp"), hidden_all.shape[1], -1).astype(
                jnp.bfloat16
            ),
            "tp",
            scatter_dimension=0,
            tiled=True,
        ).astype(jnp.float32)
    )


def per_device(
    queries,
    keys,
    values,
    stop_bias,
    out_weight,
    mix_gain,
    moe_input,
    ffn_gain,
    expert_ids,
    expert_scores,
    gate_weight,
    up_weight,
    down_weight,
):
    span = queries.shape[0]
    heads = stop_bias.shape[1]
    width_heads = queries.shape[1]
    blocks = lax.axis_size("ep")
    own_first = lax.axis_index("ep") * span
    query_heads = queries.reshape(span, heads, -1)
    query_place = own_first + jnp.arange(span)

    def piece_rows(piece, index):
        return tuple((lax.dynamic_slice_in_dim(member, index * span, span, 0) for member in piece))

    start_state = (
        jnp.zeros((blocks, heads, span), jnp.float32),
        jnp.zeros((blocks, span, width_heads), jnp.float32),
    )
    piece = (
        lax.all_gather(keys, "ep", axis=0, tiled=True),
        lax.all_gather(values, "ep", axis=0, tiled=True),
        lax.all_gather(stop_bias, "ep", axis=0, tiled=True),
    )

    def one_block(index, state):
        key_block, value_block, bias_block = piece_rows(piece, index)
        first = index * span

        def compute(inner_state):
            totals, parts = inner_state
            scores, past, rest, later = break_terms(
                query_heads, query_place, key_block, bias_block, first
            )
            part = block_part(scores, past, rest, later, value_block, heads)
            number = first // span
            totals = lax.dynamic_update_index_in_dim(totals, later[:, :, 0], number, 0)
            parts = lax.dynamic_update_index_in_dim(parts, part, number, 0)
            return (totals, parts)

        return lax.cond(first <= own_first, compute, keep, state)

    totals, parts = lax.fori_loop(0, piece[0].shape[0] // span, one_block, start_state)
    carried = lax.cumsum(totals, axis=0, reverse=True) - totals
    factor = jnp.exp(carried).transpose(0, 2, 1)[:, :, :, None]
    attended = jnp.sum(factor * parts.reshape(blocks, span, heads, -1), axis=0).reshape(
        span, width_heads
    )
    attended = attended.astype(jnp.bfloat16)
    projected = lax.psum_scatter(
        jnp.dot(attended, out_weight, preferred_element_type=jnp.float32).astype(jnp.bfloat16),
        "tp",
        scatter_dimension=0,
        tiled=True,
    ).astype(jnp.float32)
    mixed = norm_rows(projected, mix_gain).astype(jnp.bfloat16)
    normed = norm_rows(moe_input, ffn_gain).astype(jnp.bfloat16)
    rows, top = expert_ids.shape
    experts = lax.axis_size("ep")
    capacity = 3 * rows * top // (2 * experts)
    weights = expert_scores / jnp.sum(expert_scores, axis=1, keepdims=True)
    outbound, target = dispatch_plan(normed, expert_ids, experts, capacity)
    arrived = lax.all_to_all(outbound, "ep", split_axis=0, concat_axis=0, tiled=True)
    hidden_all = expert_hidden(
        lax.all_gather(arrived, "tp", axis=0, tiled=True), gate_weight, up_weight
    )
    returned = return_rows(hidden_all, down_weight, arrived.shape[0])
    picked = returned.reshape(experts * capacity, -1)[target].reshape(rows, top, -1)
    experts_mixed = jnp.sum(picked.astype(jnp.float32) * weights[:, :, None], axis=1).astype(
        jnp.bfloat16
    )
    return (mixed, experts_mixed)


def solution(mesh):
    return jax.shard_map(
        per_device,
        mesh=mesh,
        in_specs=(
            P(("grp", "ep"), "tp"),
            P(("grp", "ep"), "tp"),
            P(("grp", "ep"), "tp"),
            P(("grp", "ep"), "tp"),
            P("tp", None),
            P(),
            P(("grp", "ep", "tp"), None),
            P(),
            P(("grp", "ep", "tp"), None),
            P(("grp", "ep", "tp"), None),
            P("ep", None, "tp"),
            P("ep", None, "tp"),
            P("ep", "tp", None),
        ),
        out_specs=(P(("grp", "ep", "tp"), None), P(("grp", "ep", "tp"), None)),
        check_vma=False,
    )
```

profile of v0, /device:TPU:0, one launch (start us, length us, event | category | flops | bytes accessed | tf_op | source)
XLA Modules:
  0.0 237.8 jit_solution(10895472620026135922)
XLA Ops:
  7.2 0.0 copy-start
  7.2 0.0 all-gather.2.cloned.1.call-start
  7.2 0.9 copy.43
  8.2 0.1 eq.29
  8.3 0.1 eq.25
  8.4 0.7 broadcast_multiply_fusion
  9.1 1.2 reduce-window.6
  10.4 0.1 slice.19
  10.4 0.1 copy.45
  10.6 0.1 copy.46
  10.7 0.1 add_bitcast_fusion
  10.7 0.1 copy.42
  10.9 0.1 mul.119
  11.0 0.0 copy-start.6
  11.0 1.4 scatter_custom_fusion
  12.5 1.2 fusion.21
  13.7 1.2 fusion.23
  15.0 0.1 concatenate.3
  15.1 3.1 %gather_fusion = bf16[384,2048]{1,0:T(8,128)(2,1)} fusion(bf16[129,2048]{1,0:T(8,128)(2,1)S(1)} %concatenate.3, s32[1024]{0:T(1024)S(1)} %pad_clamp_fusion.1), kind=kCustom, calls=%fused_computation | custom fusion | bytes 3147264 | tf_op jit(solution)/shard_map/gather | solution.py:52
  18.2 43.4 %all_to_all.10 = bf16[4,96,2048]{2,1,0:T(8,128)(2,1)} all-to-all(bf16[4,96,2048]{2,1,0:T(8,128)(2,1)} %bitcast.67), channel_id=1, replica_groups=mesh['grp'=2,'ep'=4,'tp'=4] {'ep'}, dimensions={0} | all-to-all | bytes 3145728 | tf_op jit(solution)/shard_map/all_to_all | solution.py:157
  61.6 0.0 all-gather.2.cloned.1.call-update
  61.7 0.0 reduce-scatter.5.cloned.1.call-start
  61.7 45.6 %all-gather.2.cloned.1.call-done = bf16[16,96,2048]{2,1,0:T(8,128)(2,1)} async-done(((bf16[4,96,2048]{2,1,0:T(8,128)(2,1)}), bf16[16,96,2048]{2,1,0:T(8,128)(2,1)}) %all-gather.2.cloned.1.call-update) | async-done | bytes 6291472 | tf_op jit(solution)/shard_map/all_gather | solution.py:159
  107.3 4.8 %fusion.26 = f32[1536,256]{1,0:T(8,128)S(1)} fusion(bf16[1536,2048]{1,0:T(8,128)(2,1)} %bitcast.76, bf16[1,2048,256]{2,1,0:T(8,128)(2,1)S(1)} %copy-done.11), kind=kOutput, calls=%fused_computation.45 | convolution fusion | flops 1610612736 | bytes 8912896 | tf_op jit(solution)/shard_map/dot_general | solution.py:57
  112.1 0.0 copy-done.12
  112.2 2.1 fusion.18
  114.3 0.0 copy-done.1
  114.3 4.5 %convolution_convert_fusion = bf16[16,96,2048]{2,1,0:T(8,128)(2,1)} fusion(bf16[16,96,256]{2,1,0:T(8,128)(2,1)S(1)} %bitcast.70, bf16[1,256,2048]{2,1,0:T(8,128)(2,1)S(1)} %copy-done.1), kind=kOutput, calls=%fused_computation.30 | convolution fusion | flops 1613758464 | bytes 8126464 | tf_op jit(solution)/shard_map/dot_general | solution.py:71
  118.8 0.0 reduce-scatter.5.cloned.1.call-update
  118.8 0.9 copy-done.2
  119.7 0.1 copy.39
  119.8 0.1 copy.41
  119.9 0.1 copy.40
  120.1 0.0 copy-done.9
  120.1 12.6 %all_gather.13 = bf16[512,8]{0,1:T(8,128)(2,1)} all-gather(bf16[128,8]{0,1:T(8,128)(2,1)S(1)} %copy-done.9), channel_id=1, replica_groups=mesh['grp'=2,'ep'=4,'tp'=4] {'ep'}, dimensions={0}, use_global_device_ids=true | all-gather | bytes 10240 | tf_op jit(solution)/shard_map/all_gather | solution.py:117
  132.7 14.4 %all_gather.12 = bf16[512,512]{0,1:T(8,128)(2,1)S(1)} all-gather(bf16[128,512]{0,1:T(8,128)(2,1)S(1)} %copy.39), channel_id=1, replica_groups=mesh['grp'=2,'ep'=4,'tp'=4] {'ep'}, dimensions={0}, use_global_device_ids=true | all-gather | bytes 655360 | tf_op jit(solution)/shard_map/all_gather | solution.py:115
  147.1 15.3 %all_gather.14 = bf16[512,512]{0,1:T(8,128)(2,1)} all-gather(bf16[128,512]{0,1:T(8,128)(2,1)S(1)} %copy.41), channel_id=1, replica_groups=mesh['grp'=2,'ep'=4,'tp'=4] {'ep'}, dimensions={0}, use_global_device_ids=true | all-gather | bytes 655360 | tf_op jit(solution)/shard_map/all_gather | solution.py:116
  162.5 1.1 broadcast_in_dim.57
  163.6 5.2 %while.17 = (s32[]{:T(128)}, f32[4,8,128]{2,1,0:T(8,128)S(1)}, f32[4,128,512]{1,2,0:T(8,128)}, s32[]{:T(128)}, bf16[512,512]{0,1:T(8,128)(2,1)S(1)}, /*index=5*/...) while((s32[]{:T(128)}, f32[4,8,128]{2,1,0:T(8,128)S(1)}, ...), condition=%wide.region_4.5_spmd.clone.clone, body=%wide.region_0.4_spmd.clone.clone.sunk | while | flops 54150424 | bytes 4920792 | solution.py:137
  163.6 5.2 %conditional.4 = ((f32[4,8,128]{2,1,0:T(8,128)S(1)}, f32[4,128,512]{1,2,0:T(8,128)})) conditional(s32[]{:T(128)} %convert_element_type.103, (f32[4,8,128]{2,1,0:T(8,128)S(1)}, f32[4,128,512]{1,2,0:T(8,128)}) %tuple.63, (s32[]{:T(128)}, s32[]{:T(128)}, bf16[512,512]{0,1:T(8,128)(2,1)S(1)}, bf16[128,8,64]{0,2,1:T(8,128)(2,1)S(1)}, ...), branch_computations={%region_1.0_spmd, %region_2.3_spmd} | conditional | flops 54150420 | bytes 4920065 | solution.py:135
  163.6 0.9 constant_dynamic-slice_fusion
  164.5 0.7 convert_bitcast_fusion
  165.2 0.1 broadcast_compare_fusion
  165.3 0.6 fusion.5
  165.9 1.3 fusion.11
  167.2 0.9 fusion.13
  168.1 0.7 bitcast_dynamic-update-slice_fusion
  168.9 9.0 %reduce-scatter.5.cloned.1.call-done = bf16[4,96,2048]{2,1,0:T(8,128)(2,1)} async-done(((bf16[16,96,2048]{2,1,0:T(8,128)(2,1)}), bf16[4,96,2048]{2,1,0:T(8,128)(2,1)}) %reduce-scatter.5.cloned.1.call-update) | async-done | bytes 1572880 | tf_op jit(solution)/shard_map/reduce_scatter | solution.py:73
  177.8 8.0 %all-to-all-start.1 = ((bf16[4,96,2048]{2,1,0:T(8,128)(2,1)}), bf16[4,96,2048]{2,1,0:T(8,128)(2,1)}, u32[]{:S(2)}, u32[]{:S(2)}) async-start(bf16[4,96,2048]{2,1,0:T(8,128)(2,1)} %reduce-scatter.5.cloned.1.call-done), calls=%async_computation.3 | async-start | bytes 3145728 | tf_op jit(solution)/shard_map/all_to_all | solution.py:64
  185.8 0.1 fusion.20
  185.9 1.3 fusion.28
  187.2 0.0 copy-start.8
  187.2 0.0 copy-start.7
  187.2 0.0 copy-start.5
  187.2 1.3 convolution_convert_fusion.1
  188.5 0.0 reduce-scatter.3.cloned.1.call-update
  188.6 0.1 copy.47
  188.7 23.1 %reduce-scatter.3.cloned.1.call-done = bf16[32,2048]{1,0:T(8,128)(2,1)} async-done(((bf16[128,2048]{1,0:T(8,128)(2,1)}), bf16[32,2048]{1,0:T(8,128)(2,1)}) %reduce-scatter.3.cloned.1.call-update) | async-done | bytes 131088 | tf_op jit(solution)/shard_map/reduce_scatter | solution.py:144
  211.8 1.0 fusion.29
  212.9 1.7 fusion.31
  214.5 4.8 %all-to-all-done.1 = bf16[4,96,2048]{2,1,0:T(8,128)(2,1)} async-done(((bf16[4,96,2048]{2,1,0:T(8,128)(2,1)}), bf16[4,96,2048]{2,1,0:T(8,128)(2,1)}, u32[]{:S(2)}, u32[]{:S(2)}) %all-to-all-start.1) | async-done | bytes 1572896 | tf_op jit(solution)/shard_map/all_to_all | solution.py:64
  219.3 4.0 %gather_fusion.1 = bf16[256,2048]{1,0:T(8,128)(2,1)S(1)} fusion(bf16[384,2048]{1,0:T(8,128)(2,1)} %bitcast.21, s32[1024]{0:T(1024)S(1)} %pad_clamp_fusion), kind=kCustom, calls=%fused_computation.1 | custom fusion | bytes 2098176 | tf_op jit(solution)/shard_map/gather | solution.py:162
  223.3 2.4 reshape.145
  225.7 5.6 %multiply_reduce_fusion = bf16[128,2048]{1,0:T(8,128)(2,1)} fusion(f32[128,2,2048]{2,1,0:T(2,128)} %reshape.145, f32[128,2]{1,0:T(8,128)S(1)} %copy.47), kind=kLoop, calls=%fused_computation.34 | loop fusion | flops 786432 | bytes 2622464 | tf_op jit(solution)/shard_map/reduce_sum | solution.py:163
  (41 shorter events, 0.2 us)
Async XLA Ops:
  7.2 180.0 %copy-start = (bf16[512,2048]{1,0:T(8,128)(2,1)S(1)}, bf16[512,2048]{1,0:T(8,128)(2,1)}, u32[]{:S(2)}) copy-start(bf16[512,2048]{1,0:T(8,128)(2,1)} %param.21) | copy-start | bytes 6291460
  7.2 100.2 %all-gather.2.cloned.1.call-start = ((), (), s32[]{:S(2)}) async-start(), calls=%async_computation.5 | async-start | bytes 7864320 | tf_op jit(solution)/shard_map/all_gather | solution.py:159
  11.0 2.7 %copy-start.6 = (s32[256,1]{0,1:T(1,128)}, s32[256,1]{0,1:T(1,128)S(1)}, u32[]{:S(2)}) copy-start(s32[256,1]{0,1:T(1,128)S(1)} %compare_select_fusion.2) | copy-start | bytes 3076
  61.6 45.7 %copy-start.11 = (bf16[1,2048,256]{2,1,0:T(8,128)(2,1)S(1)}, bf16[1,2048,256]{2,1,0:T(8,128)(2,1)}, u32[]{:S(2)}) copy-start(bf16[1,2048,256]{2,1,0:T(8,128)(2,1)} %param.27) | copy-start | bytes 3145732
  61.7 116.1 %reduce-scatter.5.cloned.1.call-start = ((), (), s32[]{:S(2)}) async-start(), calls=%async_computation.6 | async-start | bytes 7864320 | tf_op jit(solution)/shard_map/reduce_scatter | solution.py:73
  107.3 4.8 %copy-start.10 = (bf16[16,96,2048]{2,1,0:T(8,128)(2,1)S(1)}, bf16[16,96,2048]{2,1,0:T(8,128)(2,1)}, u32[]{:S(2)}) copy-start(bf16[16,96,2048]{2,1,0:T(8,128)(2,1)} %all-gather.2.cloned.1.call-done) | copy-start | bytes 18874372
  107.3 4.9 %copy-start.12 = (bf16[1,2048,256]{2,1,0:T(8,128)(2,1)S(1)}, bf16[1,2048,256]{2,1,0:T(8,128)(2,1)}, u32[]{:S(2)}) copy-start(bf16[1,2048,256]{2,1,0:T(8,128)(2,1)} %param.28) | copy-start | bytes 3145732
  112.2 2.1 copy-start.1
  118.8 0.9 copy-start.2
  118.8 1.0 copy-start.3
  118.8 1.2 copy-start.4
  118.8 1.3 copy-start.9
  177.8 41.5 %all-to-all-start.1 = ((bf16[4,96,2048]{2,1,0:T(8,128)(2,1)}), bf16[4,96,2048]{2,1,0:T(8,128)(2,1)}, u32[]{:S(2)}, u32[]{:S(2)}) async-start(bf16[4,96,2048]{2,1,0:T(8,128)(2,1)} %reduce-scatter.5.cloned.1.call-done), calls=%async_computation.3 | async-start | bytes 3145728 | tf_op jit(solution)/shard_map/all_to_all | solution.py:64
  185.8 26.0 %reduce-scatter.3.cloned.1.call-start = ((), (), s32[]{:S(2)}) async-start(), calls=%async_computation.4 | async-start | bytes 655360 | tf_op jit(solution)/shard_map/reduce_scatter | solution.py:144
  187.2 1.3 copy-start.8
  187.2 1.5 copy-start.7
  187.2 25.6 %copy-start.5 = (f32[2048]{0:T(1024)S(1)}, f32[2048]{0:T(1024)}, u32[]{:S(2)}) copy-start(f32[2048]{0:T(1024)} %param.22) | copy-start | bytes 24580
Sparse Core Ops, SparseCore 0:
  61.8 45.4 all-gather.1
  118.9 58.8 reduce-scatter.4
  189.7 22.1 reduce-scatter.2
where the time goes:
time: 238 us
  blocking collectives  85.8 us (36%)
  waiting for transfers between devices  82.5 us (35%)
  local copies, waits for them, and re-layouts  17 us (7%)
  other arithmetic  16.3 us (7%)
  matrix products  14 us (6%)
  between operations  14 us (6%)
  starting transfers between devices  8.07 us (3%)
    all_gather x1, waiting for transfers between devices, per_device(): lax.all_gather(arrived, 'tp', axis=0, tiled=True)  45.6 us
    all_to_all x1, blocking collectives, per_device(): lax.all_to_all(outbound, 'ep', split_axis=0, concat_axis=0, tiled=True)  43.4 us
    reduce_scatter x1, waiting for transfers between devices, per_device(): lax.psum_scatter(jnp.dot(attended, out_weight, preferred_element_type=jnp...  23.1 us
    all_gather x1, blocking collectives, per_device(): lax.all_gather(values, 'ep', axis=0, tiled=True)  15.3 us
    all_gather x1, blocking collectives, per_device(): lax.all_gather(keys, 'ep', axis=0, tiled=True)  14.4 us
    all_gather x1, blocking collectives, per_device(): lax.all_gather(stop_bias, 'ep', axis=0, tiled=True)  12.6 us
    reduce_scatter x1, waiting for transfers between devices, return_rows(): lax.psum_scatter(product.reshape(sources * lax.axis_size('tp'), hidden_al...  8.95 us
    all_to_all x1, starting transfers between devices, send_back(): lax.all_to_all(summed.astype(jnp.bfloat16), 'ep', split_axis=0, concat_ax...  7.99 us
  transfers between devices with their start and end apart: 4, of which 4 were waited for; matrix products, arithmetic and copies ran while one was open for 5% of the time, Pallas kernels for 0%

commit v1 on v0

--- a/solution.py
+++ b/solution.py
@@ -1,7 +1,15 @@
+import functools
+
 import jax
 import jax.numpy as jnp
 from jax import lax
+from jax.experimental import pallas as pl
+from jax.experimental.pallas import tpu as pltpu
 from jax.sharding import PartitionSpec as P
+
+MESH = pl.DeviceIdType.MESH
+F32 = jnp.float32
+BF16 = jnp.bfloat16
 
 
 def norm_rows(values, gain):
@@ -166,9 +174,465 @@
     return (mixed, experts_mixed)
 
 
+def contract_rows(left, right):
+    return lax.dot_general(left, right, (((0,), (0,)), ((), ())), preferred_element_type=F32)
+
+
+def layer_kernel(
+    ep,
+    capacity,
+    head,
+    q_ref,
+    k_ref,
+    v_ref,
+    bias_ref,
+    ow_ref,
+    mix_gain_ref,
+    x_ref,
+    ffn_gain_ref,
+    ids_ref,
+    scores_ref,
+    g_ref,
+    u_ref,
+    d_ref,
+    mixed_ref,
+    out_ref,
+    q_all,
+    k_all,
+    v_all,
+    bias_all,
+    att_send,
+    att_all,
+    proj,
+    proj_in,
+    sel,
+    outbound,
+    rows_in,
+    acc,
+    back_out,
+    back_in,
+    g_far,
+    u_far,
+    d_far,
+    pack_send,
+    pack_recv,
+    row_send,
+    row_recv,
+    att_ssem,
+    att_rsem,
+    back_ssem,
+    back_rsem,
+    proj_ssem,
+    proj_rsem,
+    near_send,
+    near_recv,
+    x_send,
+    x_recv,
+    y_send,
+    y_recv,
+    fwd_send,
+    fwd_recv,
+):
+    me = lax.axis_index("ep")
+    tp = lax.axis_index("tp")
+    grp = lax.axis_index("grp")
+    chip, core = tp // 2, tp % 2
+    mates = [None, chip * 2 + (1 - core), (1 - chip) * 2 + core, (1 - chip) * 2 + (1 - core)]
+    span = q_ref.shape[0]
+    width = q_all.shape[2]
+    heads = width // head
+
+    barrier = pltpu.get_barrier_semaphore()
+    peers = [{"ep": lax.rem(me + r, ep)} for r in range(1, ep)]
+    peers += [{"tp": mates[m]} for m in (1, 2, 3)] + [{"grp": 1 - grp}]
+    for peer in peers:
+        pl.semaphore_signal(barrier, inc=1, device_id=peer, device_id_type=MESH)
+    pl.semaphore_wait(barrier, len(peers))
+
+    def send(src, dst, ssem, rsem, peer):
+        return pltpu.make_async_remote_copy(
+            src_ref=src,
+            dst_ref=dst,
+            send_sem=ssem,
+            recv_sem=rsem,
+            device_id=peer,
+            device_id_type=MESH,
+        )
+
+    weights = (g_ref, u_ref, d_ref)
+    fars = (g_far, u_far, d_far)
+    started = []
+
+    def go(copy):
+        copy.start()
+        started.append(copy)
+        return copy
+
+    chunks = [(c, a) for c in range(g_ref.shape[1]) for a in range(3)]
+    over_x = {}
+    for n, (c, a) in enumerate(chunks):
+        over_x[n] = go(
+            send(
+                weights[a].at[grp, c],
+                fars[a].at[1, grp, c],
+                x_send.at[n],
+                x_recv.at[n],
+                {"tp": mates[2]},
+            )
+        )
+    near = [
+        go(
+            send(
+                weights[a], fars[a].at[0], near_send.at[a], near_recv.at[a], {"tp": mates[1]}
+            )
+        )
+        for a in range(3)
+    ]
+    packs = {}
+    for r in (2, 1, 3)[: ep - 1]:
+        dest = lax.rem(me + r, ep)
+        cols = pl.ds(pl.multiple_of(dest * width, width), width)
+        pieces = (
+            (q_ref.at[:, cols], q_all.at[me]),
+            (k_ref.at[:, cols], k_all.at[me]),
+            (v_ref.at[:, cols], v_all.at[me]),
+            (bias_ref.at[dest], bias_all.at[me]),
+        )
+        packs[r] = [
+            go(send(s, t, pack_send.at[r, n], pack_recv.at[r, n], {"ep": dest}))
+            for n, (s, t) in enumerate(pieces)
+        ]
+    values = x_ref[...].astype(F32)
+    scale = lax.rsqrt(jnp.mean(values * values, axis=-1, keepdims=True) + 1e-06)
+    normed = (values * scale * ffn_gain_ref[...]).astype(BF16)
+    tokens = x_ref.shape[0]
+    ids = ids_ref[...]
+    square = (tokens, tokens)
+    lane = lax.broadcasted_iota(jnp.int32, square, 1)
+    sub = lax.broadcasted_iota(jnp.int32, square, 0)
+    named = jnp.zeros(square, F32)
+    for r in range(ep):
+        e = lax.rem(me + r, ep)
+        hit = jnp.max((ids == e).astype(F32), axis=1, keepdims=True)
+        named = named + jnp.where(lane == r, hit, 0.0)
+    named = named.astype(BF16)
+    place = contract_rows(named, (sub < lane).astype(BF16))
+    present = contract_rows(named, (sub == lane).astype(BF16))
+    slot = lax.broadcasted_iota(jnp.int32, (capacity, tokens), 0).astype(F32)
+    rows = {}
+    for r in (2, 1, 3, 0):
+        chosen = jnp.where(
+            slot == place[r : r + 1, :], present[r : r + 1, :], 0.0
+        ).astype(BF16)
+        sel[r] = chosen
+        picked = jnp.dot(chosen, normed, preferred_element_type=F32).astype(BF16)
+        if r == 0:
+            rows_in[0] = picked
+        else:
+            outbound[r] = picked
+            rows[r] = go(
+                send(
+                    outbound.at[r],
+                    rows_in.at[r],
+                    row_send.at[r],
+                    row_recv.at[r],
+                    {"ep": lax.rem(me + r, ep)},
+                )
+            )
+    own = pl.ds(pl.multiple_of(me * width, width), width)
+    q_all[me] = q_ref[:, own]
+    k_all[me] = k_ref[:, own]
+    v_all[me] = v_ref[:, own]
+    bias_all[me] = bias_ref[me]
+
+    over_y, cross = {}, {}
+
+    def forward(n):
+        c, a = chunks[n]
+        over_x[n].wait_recv()
+        over_y[n] = go(
+            send(
+                fars[a].at[1, grp, c],
+                fars[a].at[1, grp, c],
+                y_send.at[n],
+                y_recv.at[n],
+                {"grp": 1 - grp},
+            )
+        )
+        cross[0, n] = go(
+            send(
+                fars[a].at[1, grp, c],
+                fars[a].at[2, grp, c],
+                fwd_send.at[0, n],
+                fwd_recv.at[0, n],
+                {"tp": mates[1]},
+            )
+        )
+
+    def forward_again(n):
+        c, a = chunks[n]
+        over_y[n].wait_recv()
+        cross[1, n] = go(
+            send(
+                fars[a].at[1, 1 - grp, c],
+                fars[a].at[2, 1 - grp, c],
+                fwd_send.at[1, n],
+                fwd_recv.at[1, n],
+                {"tp": mates[1]},
+            )
+        )
+
+    forward(0)
+    for r in packs:
+        for copy in packs[r]:
+            copy.wait_recv()
+
+    block = (span, span)
+    key_sub = lax.broadcasted_iota(jnp.int32, block, 0)
+    key_lane = lax.broadcasted_iota(jnp.int32, block, 1)
+    after = (key_sub > key_lane).astype(BF16)
+
+    def attend(i):
+        def one(step, state):
+            j = i - step
+            past = (j * span + key_lane) < (i * span + key_sub)
+            result = []
+            for h in range(heads):
+                total, carry = state[2 * h], state[2 * h + 1]
+                cols = slice(h * head, (h + 1) * head)
+                z = lax.dot_general(
+                    q_all[i][:, cols],
+                    k_all[j][:, cols],
+                    (((1,), (1,)), ((), ())),
+                    preferred_element_type=F32,
+                )
+                z = z * head ** (-0.5) + bias_all[j][h : h + 1, :]
+                soft = jnp.log1p(jnp.exp(-jnp.abs(z)))
+                stay = -(jnp.maximum(z, 0.0) + soft)
+                stop = jnp.minimum(z, 0.0) - soft
+                rest = jnp.where(past, stay, 0.0)
+                hi = rest.astype(BF16)
+                left = rest - hi.astype(F32)
+                mid = left.astype(BF16)
+                low = (left - mid.astype(F32)).astype(BF16)
+                stack = jnp.concatenate([hi, mid, low], axis=0)
+                sums = jnp.dot(stack, after, preferred_element_type=F32)
+                within = sums[:span] + sums[span : 2 * span] + sums[2 * span :]
+                local = jnp.where(past, jnp.exp(stop + within), 0.0).astype(BF16)
+                part = jnp.dot(local, v_all[j][:, cols], preferred_element_type=F32)
+                total = total + jnp.exp(carry) * part
+                carry = carry + jnp.sum(rest, axis=1, keepdims=True)
+                result += [total, carry]
+            return tuple(result)
+
+        start = (jnp.zeros((span, head), F32), jnp.zeros((span, 1), F32)) * heads
+        state = lax.fori_loop(0, i + 1, one, start)
+        return jnp.concatenate([state[2 * h] for h in range(heads)], axis=1).astype(BF16)
+
+    att = {}
+    pending = list(range(1, len(chunks)))
+    for r in (2, 1, 3, 0):
+        dest = lax.rem(me + r, ep)
+        got = attend(dest)
+        if r == 0:
+            att_all[me] = got
+        else:
+            att_send[r] = got
+            att[r] = go(
+                send(att_send.at[r], att_all.at[me], att_ssem.at[r], att_rsem.at[r], {"ep": dest})
+            )
+        if pending:
+            forward(pending.pop(0))
+    for copy in near:
+        copy.wait_recv()
+    again = 0
+    while pending:
+        forward(pending.pop(0))
+        forward_again(again)
+        again += 1
+
+    for r in rows:
+        rows[r].wait_recv()
+    deep = rows_in.shape[2]
+
+    def hidden(g, u):
+        flat = rows_in[...].reshape(ep * capacity, deep)
+        gate = jnp.dot(flat, g.reshape(deep, -1), preferred_element_type=F32)
+        up = jnp.dot(flat, u.reshape(deep, -1), preferred_element_type=F32)
+        return (gate / (1.0 + jnp.exp(-gate)) * up).astype(BF16)
+
+    def lower(h, d):
+        return jnp.dot(h, d.reshape(-1, deep), preferred_element_type=F32)
+
+    acc[...] = lower(hidden(g_ref[...], u_ref[...]), d_ref[...])
+    acc[...] += lower(hidden(g_far[0], u_far[0]), d_far[0])
+    while again < len(chunks):
+        forward_again(again)
+        again += 1
+    acc[...] += lower(hidden(g_far[1], u_far[1]), d_far[1])
+    for n in range(len(chunks)):
+        cross[0, n].wait_recv()
+        cross[1, n].wait_recv()
+    last = hidden(g_far[2], u_far[2])
+    back = {}
+    for r in (2, 1, 3, 0):
+        piece = slice(r * capacity, (r + 1) * capacity)
+        final = (acc[piece, :] + lower(last[piece], d_far[2])).astype(BF16)
+        if r == 0:
+            back_in[0] = final
+        else:
+            back_out[r] = final
+            back[r] = go(
+                send(
+                    back_out.at[r],
+                    back_in.at[r],
+                    back_ssem.at[r],
+                    back_rsem.at[r],
+                    {"ep": lax.rem(me + ep - r, ep)},
+                )
+            )
+    for r in att:
+        att[r].wait_recv()
+    attended = jnp.concatenate([att_all[j] for j in range(ep)], axis=1)
+    share = mixed_ref.shape[0]
+    term = jnp.dot(attended, ow_ref[...], preferred_element_type=F32).astype(BF16)
+    proj[...] = term.reshape(proj.shape)
+    shares = [
+        go(send(proj.at[mates[m]], proj_in.at[m], proj_ssem.at[m], proj_rsem.at[m], {"tp": mates[m]}))
+        for m in (2, 3, 1)
+    ]
+    whole = proj[tp].astype(F32)
+    for copy in shares:
+        copy.wait_recv()
+    for m in (1, 2, 3):
+        whole = whole + proj_in[m].astype(F32)
+    scale = lax.rsqrt(jnp.mean(whole * whole, axis=-1, keepdims=True) + 1e-06)
+    mixed_ref[...] = (whole * scale * mix_gain_ref[...]).astype(BF16)
+    scores = scores_ref[...]
+    gates = scores / jnp.sum(scores, axis=1, keepdims=True)
+    result = jnp.zeros((tokens, deep), F32)
+    for r in (0, 1, 3, 2):
+        if r:
+            back[r].wait_recv()
+        e = lax.rem(me + r, ep)
+        weight = jnp.sum(jnp.where(ids == e, gates, 0.0), axis=1, keepdims=True)
+        result = result + weight * contract_rows(sel[r], back_in[r])
+    out_ref[...] = result.astype(BF16)
+    for copy in started:
+        copy.wait_send()
+
+
+def fused_device(
+    groups,
+    ep,
+    tp,
+    queries,
+    keys,
+    values,
+    stop_bias,
+    out_weight,
+    mix_gain,
+    moe_input,
+    ffn_gain,
+    expert_ids,
+    expert_scores,
+    gate_weight,
+    up_weight,
+    down_weight,
+):
+    span, cols = queries.shape
+    tokens, deep = moe_input.shape
+    top = expert_ids.shape[1]
+    capacity = 3 * tokens * top // (2 * ep)
+    width = cols // ep
+    heads = stop_bias.shape[1]
+    own_heads = heads // ep
+    units = gate_weight.shape[2]
+    cuts = 2
+    bias = stop_bias.T.astype(F32).reshape(ep, own_heads, span)
+    bias = jnp.pad(bias, ((0, 0), (0, -own_heads % 8), (0, 0)))
+    gate = gate_weight.reshape(groups, cuts, deep // (groups * cuts), units)
+    up = up_weight.reshape(gate.shape)
+    down = down_weight.reshape(groups, cuts, units // (groups * cuts), deep)
+    chunks = 3 * cuts
+    vmem = pl.BlockSpec(memory_space=pltpu.VMEM)
+    dma = pltpu.SemaphoreType.DMA
+    return pl.pallas_call(
+        functools.partial(layer_kernel, ep, capacity, cols // heads),
+        out_shape=(
+            jax.ShapeDtypeStruct((span // tp, deep), BF16),
+            jax.ShapeDtypeStruct((tokens, deep), BF16),
+        ),
+        in_specs=[vmem] * 13,
+        out_specs=(vmem, vmem),
+        scratch_shapes=[
+            pltpu.VMEM((ep, span, width), BF16),
+            pltpu.VMEM((ep, span, width), BF16),
+            pltpu.VMEM((ep, span, width), BF16),
+            pltpu.VMEM((ep,) + bias.shape[1:], F32),
+            pltpu.VMEM((ep, span, width), BF16),
+            pltpu.VMEM((ep, span, width), BF16),
+            pltpu.VMEM((tp, span // tp, deep), BF16),
+            pltpu.VMEM((tp, span // tp, deep), BF16),
+            pltpu.VMEM((ep, capacity, tokens), BF16),
+            pltpu.VMEM((ep, capacity, deep), BF16),
+            pltpu.VMEM((ep, capacity, deep), BF16),
+            pltpu.VMEM((ep * capacity, deep), F32),
+            pltpu.VMEM((ep, capacity, deep), BF16),
+            pltpu.VMEM((ep, capacity, deep), BF16),
+            pltpu.VMEM((3,) + gate.shape, BF16),
+            pltpu.VMEM((3,) + up.shape, BF16),
+            pltpu.VMEM((3,) + down.shape, BF16),
+            dma((ep, 4)),
+            dma((ep, 4)),
+            dma((ep,)),
+            dma((ep,)),
+            dma((ep,)),
+            dma((ep,)),
+            dma((ep,)),
+            dma((ep,)),
+            dma((tp,)),
+            dma((tp,)),
+            dma((3,)),
+            dma((3,)),
+            dma((chunks,)),
+            dma((chunks,)),
+            dma((chunks,)),
+            dma((chunks,)),
+            dma((2, chunks)),
+            dma((2, chunks)),
+        ],
+        compiler_params=pltpu.CompilerParams(
+            collective_id=0, has_side_effects=True, vmem_limit_bytes=60 * 2**20
+        ),
+    )(
+        queries,
+        keys,
+        values,
+        bias,
+        out_weight,
+        mix_gain.reshape(1, deep),
+        moe_input,
+        ffn_gain.reshape(1, deep),
+        expert_ids,
+        expert_scores,
+        gate,
+        up,
+        down,
+    )
+
+
+def pick_plan(groups, ep, tp, *args):
+    heads = args[3].shape[1]
+    width = args[0].shape[1] // ep
+    if groups == 2 and tp == 4 and ep == 4 and heads % ep == 0 and width % 128 == 0:
+        return fused_device(groups, ep, tp, *args)
+    return per_device(*args)
+
+
 def solution(mesh):
     return jax.shard_map(
-        per_device,
+        functools.partial(pick_plan, mesh.shape["grp"], mesh.shape["ep"], mesh.shape["tp"]),
         mesh=mesh,
         in_specs=(
             P(("grp", "ep"), "tp"),

time: 238 us -> 104 us (0.44)
  Pallas kernels: 0 us -> 95.3 us
  blocking collectives: 85.8 us -> 0 us
  waiting for transfers between devices: 82.5 us -> 0 us
  other arithmetic: 16.3 us -> 1.28 us
  matrix products: 14 us -> 0 us
  between operations: 14 us -> 0.64 us
  local copies, waits for them, and re-layouts: 17 us -> 6.27 us
  starting transfers between devices: 8.07 us -> 0 us
    pallas_call x0 -> x1, Pallas kernels: none -> 95.3 us  [fused_device(): pl.pallas_call(functools.partial(layer_kernel, ep, capacity, cols // head...]
    all_gather x1 -> x0, waiting for transfers between devices: 45.6 us -> none  [per_device(): lax.all_gather(arrived, 'tp', axis=0, tiled=True)]
    all_to_all x1 -> x0, blocking collectives: 43.4 us -> none  [per_device(): lax.all_to_all(outbound, 'ep', split_axis=0, concat_axis=0, tiled=True)]
    all_gather x3 -> x0, blocking collectives: 42.4 us -> none  [the longest x1 15.3 us: per_device(): lax.all_gather(values, 'ep', axis=0, tiled=True)]
    reduce_scatter x2 -> x0, waiting for transfers between devices: 32.1 us -> none  [the longest x1 23.1 us: per_device(): lax.psum_scatter(jnp.dot(attended, out_weight, preferred_element_type=jnp...]
    dot_general x6 -> x0, matrix products: 14 us -> none  [the longest x1 4.79 us: expert_hidden(): gate = jnp.dot(flat, gate_weight[0], preferred_element_type=jnp.float32)]
    reduce_sum x6 -> x0, other arithmetic: 9.19 us -> none  [the longest x1 5.59 us: per_device(): jnp.sum(picked.astype(jnp.float32) * weights[:, :, None], axis=1)]
    all_to_all x1 -> x0, starting transfers between devices: 7.99 us -> none  [send_back(): lax.all_to_all(summed.astype(jnp.bfloat16), 'ep', split_axis=0, concat_ax...]
  transfers between devices with their start and end apart: 4 -> 0, of which waited for: 4 -> 0; matrix products, arithmetic and copies ran while one was open for 5% -> 0% of each run, Pallas kernels for 0% -> 0%
where the time goes in v1:
time: 104 us; the launch traced here: 103 us
  Pallas kernels  95.3 us (92%)
  local copies, waits for them, and re-layouts  6.27 us (6%)
  other arithmetic  1.28 us (1%)
    pallas_call x1, Pallas kernels, fused_device(): pl.pallas_call(functools.partial(layer_kernel, ep, capacity, cols // head...  95.3 us
    unnamed x4, local copies, waits for them, and re-layouts  6.27 us

profile of v1, /device:TPU:0, one launch (start us, length us, event | category | flops | bytes accessed | tf_op | source)
XLA Modules:
  0.0 103.5 jit_solution(7274055820732571703)
XLA Ops:
  0.6 1.3 %pad_convert_fusion.bias_ref = f32[4,8,128]{2,1,0:T(8,128)} fusion(bf16[4,2,128]{2,1,0:T(2,128)(2,1)} %bitcast.13), kind=kLoop, calls=%fused_computation | loop fusion | flops 4096 | bytes 18432 | tf_op jit(solution)/shard_map/jit(_pad)/pad | solution.py:553
  1.9 1.4 %copy.15.ids_ref = s32[128,2]{1,0:T(8,128)} copy(s32[128,2]{0,1:T(2,128)} %param.21) | data formatting | bytes 2048 | tf_op args[8]
  3.3 1.4 %copy.16.scores_ref = f32[128,2]{1,0:T(8,128)} copy(f32[128,2]{0,1:T(2,128)} %param.22) | data formatting | bytes 2048 | tf_op args[9]
  4.7 95.3 %shard_map.140 = (bf16[32,2048]{1,0:T(8,128)(2,1)}, bf16[128,2048]{1,0:T(8,128)(2,1)}) custom-call(bf16[128,512]{1,0:T(8,128)(2,1)} %q_ref.1, bf16[128,512]{1,0:T(8,128)(2,1)} %k_ref.1, bf16[128,512]{1,0:T(8,128)(2,1)} %v_ref.1, f32[4,8,128]{2,1,0:T(8,128)} %pad_convert_fusion.bias_ref, bf16[512,2048]{1,0:T(8,128)(2,1)} %ow_ref.1, f32[1,2048]{1,0:T(1,128)} %bitcast.11, ...), custom_call_target="tpu_custom_call" | custom-call | tf_op jit(solution)/shard_map/pallas_call | solution.py:560
  100.0 1.6 %copy.19 = bf16[32,2048]{1,0:T(8,128)(2,1)} copy(bf16[32,2048]{1,0:T(8,128)(2,1)} %get-tuple-element.4) | data formatting | bytes 262144
  101.6 1.9 %copy.20 = bf16[128,2048]{1,0:T(8,128)(2,1)} copy(bf16[128,2048]{1,0:T(8,128)(2,1)} %get-tuple-element.5) | data formatting | bytes 1048576

commit v2 on v1

--- a/solution.py
+++ b/solution.py
@@ -201,27 +201,50 @@
     k_all,
     v_all,
     bias_all,
+    bias_rows,
     att_send,
     att_all,
     proj,
     proj_in,
+    ow,
+    meta,
+    meta_in,
+    normed_ref,
+    dense_in,
     sel,
+    gate_cols,
     outbound,
+    relay_out,
     rows_in,
     acc,
     back_out,
     back_in,
+    outer_out,
+    outer_in,
+    dense_out,
+    dense_back,
     g_far,
     u_far,
     d_far,
+    ow_sem,
     pack_send,
     pack_recv,
     row_send,
     row_recv,
+    meta_send,
+    meta_recv,
+    dense_send,
+    dense_recv,
+    relay_send,
+    relay_recv,
     att_ssem,
     att_rsem,
     back_ssem,
     back_rsem,
+    outer_send,
+    outer_recv,
+    home_send,
+    home_recv,
     proj_ssem,
     proj_rsem,
     near_send,
@@ -242,6 +265,14 @@
     width = q_all.shape[2]
     heads = width // head
 
+    half = me // 2
+    inner = lax.rem(me + 1, ep) >= 2
+    side = me + 1 - 2 * (me % 2)
+    far_inner = 2 - half
+    far_base = 2 * (1 - half)
+    ow_copy = pltpu.make_async_copy(ow_ref, ow, ow_sem)
+    ow_copy.start()
+
     barrier = pltpu.get_barrier_semaphore()
     peers = [{"ep": lax.rem(me + r, ep)} for r in range(1, ep)]
     peers += [{"tp": mates[m]} for m in (1, 2, 3)] + [{"grp": 1 - grp}]
@@ -268,7 +299,8 @@
         started.append(copy)
         return copy
 
-    chunks = [(c, a) for c in range(g_ref.shape[1]) for a in range(3)]
+    cuts = g_ref.shape[1]
+    chunks = [(c, a) for c in range(cuts) for a in range(2)] + [(c, 2) for c in range(cuts)]
     over_x = {}
     for n, (c, a) in enumerate(chunks):
         over_x[n] = go(
@@ -296,54 +328,109 @@
             (q_ref.at[:, cols], q_all.at[me]),
             (k_ref.at[:, cols], k_all.at[me]),
             (v_ref.at[:, cols], v_all.at[me]),
-            (bias_ref.at[dest], bias_all.at[me]),
+            (bias_ref, bias_all.at[me]),
         )
         packs[r] = [
             go(send(s, t, pack_send.at[r, n], pack_recv.at[r, n], {"ep": dest}))
             for n, (s, t) in enumerate(pieces)
         ]
+    tokens, deep = x_ref.shape
+    top = ids_ref.shape[0]
+    scores = scores_ref[...]
+    gates = scores / jnp.sum(scores, axis=0, keepdims=True)
+    meta[...] = jnp.zeros_like(meta)
+    meta[0:top] = ids_ref[...].astype(F32)
+    meta[top : 2 * top] = gates
+    go(send(meta, meta_in.at[me % 2], meta_send, meta_recv.at[me % 2], {"ep": far_inner}))
     values = x_ref[...].astype(F32)
     scale = lax.rsqrt(jnp.mean(values * values, axis=-1, keepdims=True) + 1e-06)
     normed = (values * scale * ffn_gain_ref[...]).astype(BF16)
-    tokens = x_ref.shape[0]
-    ids = ids_ref[...]
+    normed_ref[...] = normed
+    parts = dense_send.shape[0]
+    step_cols = deep // parts
+
+    def cols_of(c):
+        return slice(c * step_cols, (c + 1) * step_cols)
+
+    for c in range(parts):
+        go(
+            send(
+                normed_ref.at[:, cols_of(c)],
+                dense_in.at[me % 2, :, cols_of(c)],
+                dense_send.at[c],
+                dense_recv.at[me % 2, c],
+                {"ep": far_inner},
+            )
+        )
     square = (tokens, tokens)
     lane = lax.broadcasted_iota(jnp.int32, square, 1)
     sub = lax.broadcasted_iota(jnp.int32, square, 0)
-    named = jnp.zeros(square, F32)
-    for r in range(ep):
-        e = lax.rem(me + r, ep)
-        hit = jnp.max((ids == e).astype(F32), axis=1, keepdims=True)
-        named = named + jnp.where(lane == r, hit, 0.0)
-    named = named.astype(BF16)
-    place = contract_rows(named, (sub < lane).astype(BF16))
-    present = contract_rows(named, (sub == lane).astype(BF16))
+    earlier = (sub < lane).astype(BF16)
     slot = lax.broadcasted_iota(jnp.int32, (capacity, tokens), 0).astype(F32)
-    rows = {}
-    for r in (2, 1, 3, 0):
-        chosen = jnp.where(
-            slot == place[r : r + 1, :], present[r : r + 1, :], 0.0
-        ).astype(BF16)
-        sel[r] = chosen
-        picked = jnp.dot(chosen, normed, preferred_element_type=F32).astype(BF16)
-        if r == 0:
-            rows_in[0] = picked
-        else:
-            outbound[r] = picked
-            rows[r] = go(
-                send(
-                    outbound.at[r],
-                    rows_in.at[r],
-                    row_send.at[r],
-                    row_recv.at[r],
-                    {"ep": lax.rem(me + r, ep)},
-                )
-            )
+
+    def route(table, first, second, at):
+        named = jnp.zeros(square, F32)
+        gate = jnp.zeros(square, F32)
+        for n, e in enumerate((first, second)):
+            place_of = e.astype(F32)
+            for k in range(top):
+                hit = table[k : k + 1, :] == place_of
+                here = sub == n
+                named = named + jnp.where(here & hit, 1.0, 0.0)
+                gate = gate + jnp.where(here & hit, table[top + k : top + k + 1, :], 0.0)
+        place = jnp.dot(named.astype(BF16), earlier, preferred_element_type=F32)
+        for n in range(2):
+            sel[2 * at + n] = jnp.where(
+                slot == place[n : n + 1, :], named[n : n + 1, :], 0.0
+            ).astype(BF16)
+        gate_cols[at] = gate.T
+
+    def pick(n, block):
+        return jnp.dot(sel[n], block, preferred_element_type=F32).astype(BF16)
+
+    route(meta[...], me, side, 0)
+    outbound[...] = pick(1, normed)
+    side_rows = go(send(outbound, rows_in.at[1], row_send, row_recv, {"ep": side}))
+    rows_in[0] = pick(0, normed)
+
+    def dense_of(q, c):
+        return send(
+            normed_ref.at[:, cols_of(c)],
+            dense_in.at[q, :, cols_of(c)],
+            dense_send.at[c],
+            dense_recv.at[q, c],
+            {"ep": far_inner},
+        )
+
+    def relay_of(q, c):
+        return send(
+            relay_out.at[q, :, cols_of(c)],
+            rows_in.at[2 + q, :, cols_of(c)],
+            relay_send.at[q, c],
+            relay_recv.at[q, c],
+            {"ep": side},
+        )
+
+    def relay(c):
+        @pl.when(inner)
+        def _():
+            for q in range(2):
+                if c == 0:
+                    send(
+                        meta, meta_in.at[q], meta_send, meta_recv.at[q], {"ep": far_inner}
+                    ).wait_recv()
+                    route(meta_in[q], me, side, 1 + q)
+                dense_of(q, c).wait_recv()
+                block = dense_in[q, :, cols_of(c)]
+                relay_out[q, :, cols_of(c)] = pick(2 * (1 + q) + 1, block)
+                relay_of(q, c).start()
+                rows_in[2 + q, :, cols_of(c)] = pick(2 * (1 + q), block)
+
     own = pl.ds(pl.multiple_of(me * width, width), width)
     q_all[me] = q_ref[:, own]
     k_all[me] = k_ref[:, own]
     v_all[me] = v_ref[:, own]
-    bias_all[me] = bias_ref[me]
+    bias_all[me] = bias_ref[...]
 
     over_y, cross = {}, {}
 
@@ -386,6 +473,7 @@
     for r in packs:
         for copy in packs[r]:
             copy.wait_recv()
+    bias_rows[...] = bias_all[...].astype(F32)
 
     block = (span, span)
     key_sub = lax.broadcasted_iota(jnp.int32, block, 0)
@@ -406,7 +494,7 @@
                     (((1,), (1,)), ((), ())),
                     preferred_element_type=F32,
                 )
-                z = z * head ** (-0.5) + bias_all[j][h : h + 1, :]
+                z = z * head ** (-0.5) + bias_rows[j, pl.ds(me * heads + h, 1), :]
                 soft = jnp.log1p(jnp.exp(-jnp.abs(z)))
                 stay = -(jnp.maximum(z, 0.0) + soft)
                 stop = jnp.minimum(z, 0.0) - soft
@@ -430,7 +518,8 @@
         return jnp.concatenate([state[2 * h] for h in range(heads)], axis=1).astype(BF16)
 
     att = {}
-    pending = list(range(1, len(chunks)))
+    forwarded = 1
+    again = 0
     for r in (2, 1, 3, 0):
         dest = lax.rem(me + r, ep)
         got = attend(dest)
@@ -441,19 +530,27 @@
             att[r] = go(
                 send(att_send.at[r], att_all.at[me], att_ssem.at[r], att_rsem.at[r], {"ep": dest})
             )
-        if pending:
-            forward(pending.pop(0))
+        if r != 1:
+            forward(forwarded)
+            forwarded += 1
     for copy in near:
         copy.wait_recv()
-    again = 0
-    while pending:
-        forward(pending.pop(0))
-        forward_again(again)
-        again += 1
-
-    for r in rows:
-        rows[r].wait_recv()
-    deep = rows_in.shape[2]
+    for c in range(parts):
+        relay(c)
+        for _ in range(2):
+            forward_again(again)
+            again += 1
+        for _ in range(2):
+            forward(forwarded)
+            forwarded += 1
+
+    side_rows.wait_recv()
+
+    @pl.when(jnp.logical_not(inner))
+    def _():
+        for q in range(2):
+            for c in range(parts):
+                relay_of(q, c).wait_recv()
 
     def hidden(g, u):
         flat = rows_in[...].reshape(ep * capacity, deep)
@@ -466,41 +563,90 @@
 
     acc[...] = lower(hidden(g_ref[...], u_ref[...]), d_ref[...])
     acc[...] += lower(hidden(g_far[0], u_far[0]), d_far[0])
+    while again < 2 * cuts:
+        forward_again(again)
+        again += 1
+    third = hidden(g_far[1], u_far[1])
+    for n in range(2 * cuts):
+        cross[0, n].wait_recv()
+        cross[1, n].wait_recv()
+    last = hidden(g_far[2], u_far[2])
+    while forwarded < len(chunks):
+        forward(forwarded)
+        forwarded += 1
     while again < len(chunks):
         forward_again(again)
         again += 1
-    acc[...] += lower(hidden(g_far[1], u_far[1]), d_far[1])
-    for n in range(len(chunks)):
+    acc[...] += lower(third, d_far[1])
+    for n in range(2 * cuts, len(chunks)):
         cross[0, n].wait_recv()
         cross[1, n].wait_recv()
-    last = hidden(g_far[2], u_far[2])
-    back = {}
-    for r in (2, 1, 3, 0):
+    lowest = d_far[2].reshape(-1, deep)
+
+    def final(r, c):
         piece = slice(r * capacity, (r + 1) * capacity)
-        final = (acc[piece, :] + lower(last[piece], d_far[2])).astype(BF16)
-        if r == 0:
-            back_in[0] = final
-        else:
-            back_out[r] = final
-            back[r] = go(
-                send(
-                    back_out.at[r],
-                    back_in.at[r],
-                    back_ssem.at[r],
-                    back_rsem.at[r],
-                    {"ep": lax.rem(me + ep - r, ep)},
-                )
-            )
+        more = jnp.dot(last[piece], lowest[:, cols_of(c)], preferred_element_type=F32)
+        return (acc[piece, cols_of(c)] + more).astype(BF16)
+
+    def outer_of(q, c):
+        return send(
+            outer_out.at[q, :, cols_of(c)],
+            outer_in.at[q, :, cols_of(c)],
+            outer_send.at[q, c],
+            outer_recv.at[q, c],
+            {"ep": side},
+        )
+
+    for c in range(parts):
+        for q in range(2):
+            outer_out[q, :, cols_of(c)] = final(2 + q, c)
+
+            @pl.when(jnp.logical_not(inner))
+            def _():
+                outer_of(q, c).start()
+
+    for c in range(parts):
+        back_out[:, cols_of(c)] = final(1, c)
+    side_back = go(send(back_out, back_in.at[1], back_ssem, back_rsem, {"ep": side}))
+    for c in range(parts):
+        back_in[0, :, cols_of(c)] = final(0, c)
+
+    def home_of(q, c):
+        return send(
+            dense_out.at[q, :, cols_of(c)],
+            dense_back.at[:, cols_of(c)],
+            home_send.at[q, c],
+            home_recv.at[c],
+            {"ep": far_base + q},
+        )
+
+    def return_home(c):
+        @pl.when(inner)
+        def _():
+            for q in range(2):
+                outer_of(q, c).wait_recv()
+                mine = contract_rows(sel[2 * (1 + q)], outer_out[q, :, cols_of(c)])
+                outer = contract_rows(sel[2 * (1 + q) + 1], outer_in[q, :, cols_of(c)])
+                gate = gate_cols[1 + q]
+                dense_out[q, :, cols_of(c)] = (
+                    gate[:, 0:1] * mine + gate[:, 1:2] * outer
+                ).astype(BF16)
+                home_of(q, c).start()
+
+    return_home(0)
     for r in att:
         att[r].wait_recv()
+    ow_copy.wait()
     attended = jnp.concatenate([att_all[j] for j in range(ep)], axis=1)
     share = mixed_ref.shape[0]
-    term = jnp.dot(attended, ow_ref[...], preferred_element_type=F32).astype(BF16)
+    term = jnp.dot(attended, ow[...], preferred_element_type=F32).astype(BF16)
     proj[...] = term.reshape(proj.shape)
     shares = [
         go(send(proj.at[mates[m]], proj_in.at[m], proj_ssem.at[m], proj_rsem.at[m], {"tp": mates[m]}))
         for m in (2, 3, 1)
     ]
+    for c in range(1, parts):
+        return_home(c)
     whole = proj[tp].astype(F32)
     for copy in shares:
         copy.wait_recv()
@@ -508,18 +654,30 @@
         whole = whole + proj_in[m].astype(F32)
     scale = lax.rsqrt(jnp.mean(whole * whole, axis=-1, keepdims=True) + 1e-06)
     mixed_ref[...] = (whole * scale * mix_gain_ref[...]).astype(BF16)
-    scores = scores_ref[...]
-    gates = scores / jnp.sum(scores, axis=1, keepdims=True)
-    result = jnp.zeros((tokens, deep), F32)
-    for r in (0, 1, 3, 2):
-        if r:
-            back[r].wait_recv()
-        e = lax.rem(me + r, ep)
-        weight = jnp.sum(jnp.where(ids == e, gates, 0.0), axis=1, keepdims=True)
-        result = result + weight * contract_rows(sel[r], back_in[r])
-    out_ref[...] = result.astype(BF16)
+    gate = gate_cols[0]
+    side_back.wait_recv()
+    for c in range(parts):
+        mine = contract_rows(sel[0], back_in[0, :, cols_of(c)])
+        beside = contract_rows(sel[1], back_in[1, :, cols_of(c)])
+        acc[0:tokens, cols_of(c)] = gate[:, 0:1] * mine + gate[:, 1:2] * beside
+    for c in range(parts):
+        home_of(0, c).wait_recv()
+        out_ref[:, cols_of(c)] = (
+            acc[0:tokens, cols_of(c)] + dense_back[:, cols_of(c)].astype(F32)
+        ).astype(BF16)
     for copy in started:
         copy.wait_send()
+    for q in range(2):
+        for c in range(parts):
+
+            @pl.when(inner)
+            def _():
+                relay_of(q, c).wait_send()
+                home_of(q, c).wait_send()
+
+            @pl.when(jnp.logical_not(inner))
+            def _():
+                outer_of(q, c).wait_send()
 
 
 def fused_device(
@@ -546,11 +704,10 @@
     capacity = 3 * tokens * top // (2 * ep)
     width = cols // ep
     heads = stop_bias.shape[1]
-    own_heads = heads // ep
     units = gate_weight.shape[2]
-    cuts = 2
-    bias = stop_bias.T.astype(F32).reshape(ep, own_heads, span)
-    bias = jnp.pad(bias, ((0, 0), (0, -own_heads % 8), (0, 0)))
+    cuts = 4
+    parts = 4
+    lines = 8
     gate = gate_weight.reshape(groups, cuts, deep // (groups * cuts), units)
     up = up_weight.reshape(gate.shape)
     down = down_weight.reshape(groups, cuts, units // (groups * cuts), deep)
@@ -563,34 +720,57 @@
             jax.ShapeDtypeStruct((span // tp, deep), BF16),
             jax.ShapeDtypeStruct((tokens, deep), BF16),
         ),
-        in_specs=[vmem] * 13,
+        in_specs=[vmem] * 4 + [pl.BlockSpec(memory_space=pl.ANY)] + [vmem] * 8,
         out_specs=(vmem, vmem),
         scratch_shapes=[
             pltpu.VMEM((ep, span, width), BF16),
             pltpu.VMEM((ep, span, width), BF16),
             pltpu.VMEM((ep, span, width), BF16),
-            pltpu.VMEM((ep,) + bias.shape[1:], F32),
+            pltpu.VMEM((ep, heads, span), BF16),
+            pltpu.VMEM((ep, heads, span), F32),
             pltpu.VMEM((ep, span, width), BF16),
             pltpu.VMEM((ep, span, width), BF16),
             pltpu.VMEM((tp, span // tp, deep), BF16),
             pltpu.VMEM((tp, span // tp, deep), BF16),
-            pltpu.VMEM((ep, capacity, tokens), BF16),
-            pltpu.VMEM((ep, capacity, deep), BF16),
+            pltpu.VMEM(out_weight.shape, BF16),
+            pltpu.VMEM((lines, tokens), F32),
+            pltpu.VMEM((2, lines, tokens), F32),
+            pltpu.VMEM((tokens, deep), BF16),
+            pltpu.VMEM((2, tokens, deep), BF16),
+            pltpu.VMEM((6, capacity, tokens), BF16),
+            pltpu.VMEM((3, tokens, tokens), F32),
+            pltpu.VMEM((capacity, deep), BF16),
+            pltpu.VMEM((2, capacity, deep), BF16),
             pltpu.VMEM((ep, capacity, deep), BF16),
             pltpu.VMEM((ep * capacity, deep), F32),
-            pltpu.VMEM((ep, capacity, deep), BF16),
-            pltpu.VMEM((ep, capacity, deep), BF16),
+            pltpu.VMEM((capacity, deep), BF16),
+            pltpu.VMEM((2, capacity, deep), BF16),
+            pltpu.VMEM((2, capacity, deep), BF16),
+            pltpu.VMEM((2, capacity, deep), BF16),
+            pltpu.VMEM((2, tokens, deep), BF16),
+            pltpu.VMEM((tokens, deep), BF16),
             pltpu.VMEM((3,) + gate.shape, BF16),
             pltpu.VMEM((3,) + up.shape, BF16),
             pltpu.VMEM((3,) + down.shape, BF16),
+            dma(()),
             dma((ep, 4)),
             dma((ep, 4)),
+            dma(()),
+            dma(()),
+            dma(()),
+            dma((2,)),
+            dma((parts,)),
+            dma((2, parts)),
+            dma((2, parts)),
+            dma((2, parts)),
             dma((ep,)),
             dma((ep,)),
-            dma((ep,)),
-            dma((ep,)),
-            dma((ep,)),
-            dma((ep,)),
+            dma(()),
+            dma(()),
+            dma((2, parts)),
+            dma((2, parts)),
+            dma((2, parts)),
+            dma((parts,)),
             dma((tp,)),
             dma((tp,)),
             dma((3,)),
@@ -609,13 +789,13 @@
         queries,
         keys,
         values,
-        bias,
+        stop_bias.T,
         out_weight,
         mix_gain.reshape(1, deep),
         moe_input,
         ffn_gain.reshape(1, deep),
-        expert_ids,
-        expert_scores,
+        expert_ids.T,
+        expert_scores.T,
         gate,
         up,
         down,

time: 104 us -> 97 us (0.933); the launches traced: 103 us -> 95.4 us
  Pallas kernels: 95.3 us -> 91.3 us
  local copies, waits for them, and re-layouts: 6.27 us -> 3.45 us
  other arithmetic: 1.28 us -> 0 us
    pallas_call x1, Pallas kernels: 95.3 us -> 91.3 us  [fused_device(): pl.pallas_call(functools.partial(layer_kernel, ep, capacity, cols // head...]
    unnamed x4 -> x2, local copies, waits for them, and re-layouts: 6.27 us -> 3.45 us
    pad x1 -> x0, other arithmetic: 1.28 us -> none  [fused_device(): bias = jnp.pad(bias, ((0, 0), (0, -own_heads % 8), (0, 0)))]
where the time goes in v2:
time: 97 us; the launch traced here: 95.4 us
  Pallas kernels  91.3 us (94%)
  local copies, waits for them, and re-layouts  3.45 us (4%)
    pallas_call x1, Pallas kernels, fused_device(): pl.pallas_call(functools.partial(layer_kernel, ep, capacity, cols // head...  91.3 us
    unnamed x2, local copies, waits for them, and re-layouts  3.45 us

profile of v2, /device:TPU:0, one launch (start us, length us, event | category | flops | bytes accessed | tf_op | source)
XLA Modules:
  0.0 95.4 jit_solution(1522762220621541069)
XLA Ops:
  0.6 91.3 %shard_map.140 = (bf16[32,2048]{1,0:T(8,128)(2,1)}, bf16[128,2048]{1,0:T(8,128)(2,1)}) custom-call(bf16[128,512]{1,0:T(8,128)(2,1)} %q_ref.1, bf16[128,512]{1,0:T(8,128)(2,1)} %k_ref.1, bf16[128,512]{1,0:T(8,128)(2,1)} %v_ref.1, bf16[8,128]{1,0:T(8,128)(2,1)} %bitcast.13, bf16[512,2048]{1,0:T(8,128)(2,1)} %ow_ref.1, f32[1,2048]{1,0:T(1,128)} %bitcast.11, ...), custom_call_target="tpu_custom_call" | custom-call | tf_op jit(solution)/shard_map/pallas_call | solution.py:717
  91.9 1.6 %copy.17 = bf16[32,2048]{1,0:T(8,128)(2,1)} copy(bf16[32,2048]{1,0:T(8,128)(2,1)} %get-tuple-element.4) | data formatting | bytes 262144
  93.5 1.9 %copy.18 = bf16[128,2048]{1,0:T(8,128)(2,1)} copy(bf16[128,2048]{1,0:T(8,128)(2,1)} %get-tuple-element.5) | data formatting | bytes 1048576

commit v3 on v2

--- a/solution.py
+++ b/solution.py
@@ -320,20 +320,6 @@
         )
         for a in range(3)
     ]
-    packs = {}
-    for r in (2, 1, 3)[: ep - 1]:
-        dest = lax.rem(me + r, ep)
-        cols = pl.ds(pl.multiple_of(dest * width, width), width)
-        pieces = (
-            (q_ref.at[:, cols], q_all.at[me]),
-            (k_ref.at[:, cols], k_all.at[me]),
-            (v_ref.at[:, cols], v_all.at[me]),
-            (bias_ref, bias_all.at[me]),
-        )
-        packs[r] = [
-            go(send(s, t, pack_send.at[r, n], pack_recv.at[r, n], {"ep": dest}))
-            for n, (s, t) in enumerate(pieces)
-        ]
     tokens, deep = x_ref.shape
     top = ids_ref.shape[0]
     scores = scores_ref[...]
@@ -426,6 +412,20 @@
                 relay_of(q, c).start()
                 rows_in[2 + q, :, cols_of(c)] = pick(2 * (1 + q), block)
 
+    packs = {}
+    for r in (2, 1, 3)[: ep - 1]:
+        dest = lax.rem(me + r, ep)
+        cols = pl.ds(pl.multiple_of(dest * width, width), width)
+        pieces = (
+            (q_ref.at[:, cols], q_all.at[me]),
+            (k_ref.at[:, cols], k_all.at[me]),
+            (v_ref.at[:, cols], v_all.at[me]),
+            (bias_ref, bias_all.at[me]),
+        )
+        packs[r] = [
+            go(send(s, t, pack_send.at[r, n], pack_recv.at[r, n], {"ep": dest}))
+            for n, (s, t) in enumerate(pieces)
+        ]
     own = pl.ds(pl.multiple_of(me * width, width), width)
     q_all[me] = q_ref[:, own]
     k_all[me] = k_ref[:, own]
@@ -468,12 +468,6 @@
                 {"tp": mates[1]},
             )
         )
-
-    forward(0)
-    for r in packs:
-        for copy in packs[r]:
-            copy.wait_recv()
-    bias_rows[...] = bias_all[...].astype(F32)
 
     block = (span, span)
     key_sub = lax.broadcasted_iota(jnp.int32, block, 0)
@@ -517,9 +511,48 @@
         state = lax.fori_loop(0, i + 1, one, start)
         return jnp.concatenate([state[2 * h] for h in range(heads)], axis=1).astype(BF16)
 
+    for copy in near:
+        copy.wait_recv()
+    again = forwarded = 0
+    for c in range(parts):
+        for _ in range(2):
+            forward(forwarded)
+            forwarded += 1
+        relay(c)
+        for _ in range(2 if c else 0):
+            forward_again(again)
+            again += 1
+
+    side_rows.wait_recv()
+
+    @pl.when(jnp.logical_not(inner))
+    def _():
+        for q in range(2):
+            for c in range(parts):
+                relay_of(q, c).wait_recv()
+
+    def hidden(g, u):
+        flat = rows_in[...].reshape(ep * capacity, deep)
+        gate = jnp.dot(flat, g.reshape(deep, -1), preferred_element_type=F32)
+        up = jnp.dot(flat, u.reshape(deep, -1), preferred_element_type=F32)
+        return (gate / (1.0 + jnp.exp(-gate)) * up).astype(BF16)
+
+    def lower(h, d):
+        return jnp.dot(h, d.reshape(-1, deep), preferred_element_type=F32)
+
+    acc[...] = lower(hidden(g_ref[...], u_ref[...]), d_ref[...])
+    for _ in range(2):
+        forward_again(again)
+        again += 1
+        forward(forwarded)
+        forwarded += 1
+    acc[...] += lower(hidden(g_far[0], u_far[0]), d_far[0])
+    for r in packs:
+        for copy in packs[r]:
+            copy.wait_recv()
+    bias_rows[...] = bias_all[...].astype(F32)
+
     att = {}
-    forwarded = 1
-    again = 0
     for r in (2, 1, 3, 0):
         dest = lax.rem(me + r, ep)
         got = attend(dest)
@@ -530,40 +563,9 @@
             att[r] = go(
                 send(att_send.at[r], att_all.at[me], att_ssem.at[r], att_rsem.at[r], {"ep": dest})
             )
-        if r != 1:
+        if forwarded < len(chunks):
             forward(forwarded)
             forwarded += 1
-    for copy in near:
-        copy.wait_recv()
-    for c in range(parts):
-        relay(c)
-        for _ in range(2):
-            forward_again(again)
-            again += 1
-        for _ in range(2):
-            forward(forwarded)
-            forwarded += 1
-
-    side_rows.wait_recv()
-
-    @pl.when(jnp.logical_not(inner))
-    def _():
-        for q in range(2):
-            for c in range(parts):
-                relay_of(q, c).wait_recv()
-
-    def hidden(g, u):
-        flat = rows_in[...].reshape(ep * capacity, deep)
-        gate = jnp.dot(flat, g.reshape(deep, -1), preferred_element_type=F32)
-        up = jnp.dot(flat, u.reshape(deep, -1), preferred_element_type=F32)
-        return (gate / (1.0 + jnp.exp(-gate)) * up).astype(BF16)
-
-    def lower(h, d):
-        return jnp.dot(h, d.reshape(-1, deep), preferred_element_type=F32)
-
-    acc[...] = lower(hidden(g_ref[...], u_ref[...]), d_ref[...])
-    acc[...] += lower(hidden(g_far[0], u_far[0]), d_far[0])
-    while again < 2 * cuts:
         forward_again(again)
         again += 1
     third = hidden(g_far[1], u_far[1])
@@ -680,6 +682,11 @@
                 outer_of(q, c).wait_send()
 
 
+def settle_kernel(mixed_ref, out_ref, mixed_to, out_to):
+    mixed_to[...] = mixed_ref[...]
+    out_to[...] = out_ref[...]
+
+
 def fused_device(
     groups,
     ep,
@@ -714,7 +721,7 @@
     chunks = 3 * cuts
     vmem = pl.BlockSpec(memory_space=pltpu.VMEM)
     dma = pltpu.SemaphoreType.DMA
-    return pl.pallas_call(
+    results = pl.pallas_call(
         functools.partial(layer_kernel, ep, capacity, cols // heads),
         out_shape=(
             jax.ShapeDtypeStruct((span // tp, deep), BF16),
@@ -800,6 +807,12 @@
         up,
         down,
     )
+    return pl.pallas_call(
+        settle_kernel,
+        out_shape=tuple(jax.ShapeDtypeStruct(r.shape, r.dtype) for r in results),
+        in_specs=[vmem] * 2,
+        out_specs=(vmem, vmem),
+    )(*results)
 
 
 def pick_plan(groups, ep, tp, *args):

time: 97 us -> 93.1 us (0.960); the launches traced: 95.4 us -> 92.9 us
  local copies, waits for them, and re-layouts: 3.45 us -> 0 us
  Pallas kernels: 91.3 us -> 92.3 us
    unnamed x2 -> x0, local copies, waits for them, and re-layouts: 3.45 us -> none
    pallas_call x0 -> x1, Pallas kernels: none -> 1.96 us  [fused_device(): pl.pallas_call(settle_kernel, out_shape=tuple((jax.ShapeDtypeStruct(r.sha...]
    pallas_call x1, Pallas kernels: 91.3 us -> 90.3 us  [fused_device(): pl.pallas_call(functools.partial(layer_kernel, ep, capacity, cols // head...]
where the time goes in v3:
time: 93.1 us; the launch traced here: 92.9 us
  Pallas kernels  92.3 us (99%)
    pallas_call x1, Pallas kernels, fused_device(): pl.pallas_call(functools.partial(layer_kernel, ep, capacity, cols // head...  90.3 us
    pallas_call x1, Pallas kernels, fused_device(): pl.pallas_call(settle_kernel, out_shape=tuple((jax.ShapeDtypeStruct(r.sha...  1.96 us

profile of v3, /device:TPU:0, one launch (start us, length us, event | category | flops | bytes accessed | tf_op | source)
XLA Modules:
  0.0 92.9 jit_solution(15859741015897009023)
XLA Ops:
  0.6 90.3 %shard_map.140 = (bf16[32,2048]{1,0:T(8,128)(2,1)}, bf16[128,2048]{1,0:T(8,128)(2,1)}) custom-call(bf16[128,512]{1,0:T(8,128)(2,1)} %q_ref.1, bf16[128,512]{1,0:T(8,128)(2,1)} %k_ref.1, bf16[128,512]{1,0:T(8,128)(2,1)} %v_ref.1, bf16[8,128]{1,0:T(8,128)(2,1)} %bitcast.13, bf16[512,2048]{1,0:T(8,128)(2,1)} %ow_ref.1, f32[1,2048]{1,0:T(1,128)} %bitcast.11, ...), custom_call_target="tpu_custom_call" | custom-call | tf_op jit(solution)/shard_map/pallas_call | solution.py:724
  91.0 2.0 %shard_map.141 = (bf16[32,2048]{1,0:T(8,128)(2,1)}, bf16[128,2048]{1,0:T(8,128)(2,1)}) custom-call(bf16[32,2048]{1,0:T(8,128)(2,1)} %get-tuple-element.4.mixed_ref, bf16[128,2048]{1,0:T(8,128)(2,1)} %get-tuple-element.5.out_ref), custom_call_target="tpu_custom_call" | custom-call | tf_op jit(solution)/shard_map/pallas_call | solution.py:810
